TPU v7x, 256 devices: a 8x8x2 block of a 8x8x16 slice. The times are simulated.
256 devices in a mesh: grp: 2 (over z), fs: 16 (over y, core), tp: 8 (over x).
Axes of the slice: x: 8, y: 8, z: 2, core: 2. Of those that a mesh axis runs over, the one named last changes fastest.
The devices are a block of a 8x8x16 slice.
Arguments:
- stream: bfloat16 [32768, 2048], P(('grp', 'fs', 'tp')), parts along dimension 0, may hold values from -4 to 4
- gain_first: bfloat16 [2048], replicated, may hold values from 0.099609375 to 1.8984375
- gate_first: bfloat16 [2048, 4096], P('fs', 'tp'), may hold values from -0.125 to 0.125
- up_first: bfloat16 [2048, 4096], P('fs', 'tp'), may hold values from -0.125 to 0.125
- down_first: bfloat16 [4096, 2048], P('tp', 'fs'), may hold values from -0.09375 to 0.09375
- gain_second: bfloat16 [2048], replicated, may hold values from 0.099609375 to 1.8984375
- gate_second: bfloat16 [2048, 4096], P('fs', 'tp'), may hold values from -0.125 to 0.125
- up_second: bfloat16 [2048, 4096], P('fs', 'tp'), may hold values from -0.125 to 0.125
- down_second: bfloat16 [4096, 2048], P('tp', 'fs'), may hold values from -0.09375 to 0.09375
Outputs:
- result: bfloat16 [32768, 2048], P(('grp', 'fs', 'tp')), parts along dimension 0
There are 2 independent parts, one for each index of `grp`. A program takes and returns all parts, laid end to end along the dimension named above; an argument that names none is the same for every part. Nothing has to cross between parts.
All inputs are finite; a program needn't handle non-finite values.
Results may differ from a plain program's by a relative error of at most 0.018.
Values may be sent and summed in bfloat16 or wider, within the bound.
A program may use at most 64 MiB of HBM per device.

v0:
```python
import jax
import jax.numpy as jnp
from jax import lax
from jax.sharding import PartitionSpec as P


def gather_turned(arrays, axis, dims):
    turned = [jnp.moveaxis(a, dim, 0) for a, dim in zip(arrays, dims)]
    widths = [t[0].size for t in turned]
    both = jnp.concatenate([t.reshape(-1, w) for t, w in zip(turned, widths)], axis=1)
    result = lax.all_gather(both, axis, axis=0, tiled=True)
    blocks = jnp.split(result, [sum(widths[:k]) for k in range(1, len(widths))], axis=1)
    return tuple(
        (
            jnp.moveaxis(b.reshape(-1, *t.shape[1:]), 0, dim)
            for b, t, dim in zip(blocks, turned, dims)
        )
    )


def half_branch(stream, gain, gathered):
    stream_f = stream.astype(jnp.float32)
    normed = (
        stream_f
        * lax.rsqrt(jnp.mean(stream_f * stream_f, axis=-1, keepdims=True) + 1e-06)
        * gain.astype(jnp.float32)
    ).astype(jnp.bfloat16)
    tokens = lax.all_gather(normed, "tp", axis=0, tiled=True)
    gate_act = jnp.dot(tokens, gathered[0], preferred_element_type=jnp.float32)
    up_act = jnp.dot(tokens, gathered[1], preferred_element_type=jnp.float32)
    down_full = gathered[2]
    hidden = (jax.nn.silu(gate_act) * up_act).astype(jnp.bfloat16)
    summed = lax.psum_scatter(
        jnp.dot(hidden, down_full, preferred_element_type=jnp.float32).astype(jnp.bfloat16),
        "tp",
        scatter_dimension=0,
        tiled=True,
    ).astype(jnp.float32)
    return (stream_f + 0.5 * summed).astype(jnp.bfloat16)


def local(
    stream,
    gain_first,
    gate_first,
    up_first,
    down_first,
    gain_second,
    gate_second,
    up_second,
    down_second,
):
    weights = gather_turned(
        (gate_first, up_first, down_first, gate_second, up_second, down_second),
        "fs",
        (0, 0, 1, 0, 0, 1),
    )
    first_set = (weights[0], weights[1], weights[2])
    second_set = (weights[3], weights[4], weights[5])
    middle = half_branch(stream, gain_first, first_set)
    return half_branch(middle, gain_second, second_set)


def solution(mesh):
    in_specs = (
        P(("grp", "fs", "tp"), None),
        P(),
        P("fs", "tp"),
        P("fs", "tp"),
        P("tp", "fs"),
        P(),
        P("fs", "tp"),
        P("fs", "tp"),
        P("tp", "fs"),
    )
    out_specs = P(("grp", "fs", "tp"), None)
    return jax.shard_map(local, mesh=mesh, in_specs=in_specs, out_specs=out_specs, check_vma=False)
```

profile of v0, /device:TPU:514, one launch (start us, length us, event | category | flops | bytes accessed | tf_op | source)
XLA Modules:
  0.0 375.1 jit_solution(9833353432578024981)
XLA Ops:
  6.5 0.0 copy-start.3
  6.5 0.0 copy-start.4
  6.6 0.0 copy-start.5
  6.6 0.0 copy-start.6
  6.6 0.0 copy-start.7
  6.6 0.1 all-gather.4.cloned.1.call-start
  6.6 1.3 fusion.18
  8.0 0.0 copy-start.8
  8.0 0.7 convert_element_type.43
  8.7 2.0 fusion.20
  10.7 0.1 all-gather.4.cloned.1.call-update
  10.8 0.1 all-gather.6.cloned.1.call-start
  10.9 0.0 copy-done.3
  10.9 0.1 copy.10
  11.0 0.0 copy-done.4
  11.0 0.1 copy.11
  11.1 0.0 copy-done.5
  11.2 0.1 copy.12
  11.3 0.0 copy-done.6
  11.3 0.1 copy.13
  11.5 0.0 copy-done.7
  11.6 0.0 copy-done.8
  11.6 0.0 copy-start.2
  11.6 0.9 copy-done.2
  12.5 0.1 all-gather.6.cloned.1.call-update
  12.5 0.1 reduce-scatter.3.cloned.1.call-start
  12.6 70.5 %all-gather.4.cloned.1.call-done = bf16[1024,2048]{1,0:T(8,128)(2,1)} async-done(((bf16[128,2048]{1,0:T(8,128)(2,1)}), bf16[1024,2048]{1,0:T(8,128)(2,1)}) %all-gather.4.cloned.1.call-update) | async-done | bytes 4194320 | tf_op jit(solution)/shard_map/all_gather | solution.py:28
  83.1 85.3 %all-gather.6.cloned.1.call-done = bf16[2048,3072]{0,1:T(8,128)(2,1)} async-done(((bf16[128,3072]{0,1:T(8,128)(2,1)}), bf16[2048,3072]{0,1:T(8,128)(2,1)}) %all-gather.6.cloned.1.call-update) | async-done | bytes 12582928 | tf_op jit(solution)/shard_map/all_gather | solution.py:11
  168.4 5.2 %fusion.8 = f32[1024,512]{1,0:T(8,128)S(1)} fusion(bf16[1024,2048]{1,0:T(8,128)(2,1)} %all-gather.4.cloned.1.call-done, bf16[2048,3072]{0,1:T(8,128)(2,1)} %all-gather.6.cloned.1.call-done), kind=kOutput, calls=%fused_computation.10 | convolution fusion | flops 2147483648 | bytes 8388608 | tf_op jit(solution)/shard_map/dot_general | solution.py:29
  173.6 10.0 %convolution_convert_fusion.1 = bf16[1024,2048]{1,0:T(8,128)(2,1)} fusion(bf16[2048,3072]{0,1:T(8,128)(2,1)} %all-gather.6.cloned.1.call-done, f32[1024,512]{1,0:T(8,128)S(1)} %fusion.8, bf16[1024,2048]{1,0:T(8,128)(2,1)} %all-gather.4.cloned.1.call-done), kind=kOutput, calls=%fused_computation.1 | convolution fusion | flops 4300210176 | bytes 14680064 | tf_op jit(solution)/shard_map/dot_general | solution.py:34
  183.6 0.0 copy-start.9
  183.6 0.0 copy-start
  183.6 0.1 reduce-scatter.3.cloned.1.call-update
  183.7 0.1 all-gather.8.cloned.1.call-start
  183.8 0.5 copy-done.9
  184.3 52.8 %reduce-scatter.3.cloned.1.call-done = bf16[128,2048]{1,0:T(8,128)(2,1)} async-done(((bf16[1024,2048]{1,0:T(8,128)(2,1)}), bf16[128,2048]{1,0:T(8,128)(2,1)}) %reduce-scatter.3.cloned.1.call-update) | async-done | bytes 524304 | tf_op jit(solution)/shard_map/reduce_scatter | solution.py:33
  237.1 0.0 copy-done
  237.1 1.3 fusion.22
  238.4 2.1 fusion.24
  240.5 0.1 all-gather.8.cloned.1.call-update
  240.6 0.2 reduce-scatter.5.cloned.1.call-start
  240.8 54.7 %all-gather.8.cloned.1.call-done = bf16[1024,2048]{1,0:T(8,128)(2,1)} async-done(((bf16[128,2048]{1,0:T(8,128)(2,1)}), bf16[1024,2048]{1,0:T(8,128)(2,1)}) %all-gather.8.cloned.1.call-update) | async-done | bytes 4194320 | tf_op jit(solution)/shard_map/all_gather | solution.py:28
  295.6 5.2 %fusion.3 = f32[1024,512]{1,0:T(8,128)S(1)} fusion(bf16[1024,2048]{1,0:T(8,128)(2,1)} %all-gather.8.cloned.1.call-done, bf16[2048,3072]{0,1:T(8,128)(2,1)} %all-gather.6.cloned.1.call-done), kind=kOutput, calls=%fused_computation.5 | convolution fusion | flops 2147483648 | bytes 8388608 | tf_op jit(solution)/shard_map/dot_general | solution.py:29
  300.8 10.0 %convolution_convert_fusion = bf16[1024,2048]{1,0:T(8,128)(2,1)} fusion(bf16[2048,3072]{0,1:T(8,128)(2,1)} %all-gather.6.cloned.1.call-done, f32[1024,512]{1,0:T(8,128)S(1)} %fusion.3, bf16[1024,2048]{1,0:T(8,128)(2,1)} %all-gather.8.cloned.1.call-done), kind=kOutput, calls=%fused_computation | convolution fusion | flops 4300210176 | bytes 14680064 | tf_op jit(solution)/shard_map/dot_general | solution.py:34
  310.8 0.0 copy-start.1
  310.8 0.1 reduce-scatter.5.cloned.1.call-update
  310.9 55.6 %reduce-scatter.5.cloned.1.call-done = bf16[128,2048]{1,0:T(8,128)(2,1)} async-done(((bf16[1024,2048]{1,0:T(8,128)(2,1)}), bf16[128,2048]{1,0:T(8,128)(2,1)}) %reduce-scatter.5.cloned.1.call-update) | async-done | bytes 524304 | tf_op jit(solution)/shard_map/reduce_scatter | solution.py:33
  366.4 0.0 copy-done.1
  366.4 2.1 fusion.25
  (9 shorter events, 0.1 us)
Async XLA Ops:
  6.5 4.3 %copy-start.3 = (bf16[128,512]{1,0:T(8,128)(2,1)S(1)}, bf16[128,512]{1,0:T(8,128)(2,1)}, u32[]{:S(2)}) copy-start(bf16[128,512]{1,0:T(8,128)(2,1)} %param.11) | copy-start | bytes 393220
  6.5 4.5 %copy-start.4 = (bf16[128,512]{1,0:T(8,128)(2,1)S(1)}, bf16[128,512]{1,0:T(8,128)(2,1)}, u32[]{:S(2)}) copy-start(bf16[128,512]{1,0:T(8,128)(2,1)} %param.12) | copy-start | bytes 393220
  6.6 4.6 %copy-start.5 = (bf16[128,512]{1,0:T(8,128)(2,1)S(1)}, bf16[128,512]{1,0:T(8,128)(2,1)}, u32[]{:S(2)}) copy-start(bf16[128,512]{1,0:T(8,128)(2,1)} %param.15) | copy-start | bytes 393220
  6.6 4.7 %copy-start.6 = (bf16[128,512]{1,0:T(8,128)(2,1)S(1)}, bf16[128,512]{1,0:T(8,128)(2,1)}, u32[]{:S(2)}) copy-start(bf16[128,512]{1,0:T(8,128)(2,1)} %param.16) | copy-start | bytes 393220
  6.6 4.9 %copy-start.7 = (bf16[512,128]{1,0:T(8,128)(2,1)S(1)}, bf16[512,128]{1,0:T(8,128)(2,1)}, u32[]{:S(2)}) copy-start(bf16[512,128]{1,0:T(8,128)(2,1)} %param.13) | copy-start | bytes 393220
  6.6 76.6 %all-gather.4.cloned.1.call-start = ((), (), s32[]{:S(2)}) async-start(), calls=%async_computation.2 | async-start | bytes 4718592 | tf_op jit(solution)/shard_map/all_gather | solution.py:28
  8.0 3.6 copy-start.8
  10.8 157.6 %all-gather.6.cloned.1.call-start = ((), (), s32[]{:S(2)}) async-start(), calls=%async_computation.3 | async-start | bytes 13369344 | tf_op jit(solution)/shard_map/all_gather | solution.py:11
  11.6 0.9 copy-start.2
  12.5 224.6 %reduce-scatter.3.cloned.1.call-start = ((), (), s32[]{:S(2)}) async-start(), calls=%async_computation.4 | async-start | bytes 4718592 | tf_op jit(solution)/shard_map/reduce_scatter | solution.py:33
  183.6 0.7 copy-start.9
  183.6 53.5 %copy-start = (bf16[128,2048]{1,0:T(8,128)(2,1)S(1)}, bf16[128,2048]{1,0:T(8,128)(2,1)}, u32[]{:S(2)}) copy-start(bf16[128,2048]{1,0:T(8,128)(2,1)} %param.9) | copy-start | bytes 1572868
  183.7 111.9 %all-gather.8.cloned.1.call-start = ((), (), s32[]{:S(2)}) async-start(), calls=%async_computation.5 | async-start | bytes 4718592 | tf_op jit(solution)/shard_map/all_gather | solution.py:28
  240.6 125.9 %reduce-scatter.5.cloned.1.call-start = ((), (), s32[]{:S(2)}) async-start(), calls=%async_computation.6 | async-start | bytes 4718592 | tf_op jit(solution)/shard_map/reduce_scatter | solution.py:33
  310.8 55.6 %copy-start.1 = (bf16[128,2048]{1,0:T(8,128)(2,1)S(1)}, bf16[128,2048]{1,0:T(8,128)(2,1)}, u32[]{:S(2)}) copy-start(bf16[128,2048]{1,0:T(8,128)(2,1)} %reduce-scatter.3.cloned.1.call-done) | copy-start | bytes 1572868
Sparse Core Ops, SparseCore 0:
  10.9 72.1 all-gather.3
  84.9 83.4 all-gather.5
  183.8 53.2 reduce-scatter.2
  240.7 54.8 all-gather.7
  311.0 55.4 reduce-scatter.4
where the time goes:
time: 377 us; the launch traced here: 375 us
  waiting for transfers between devices  319 us (85%)
  matrix products  30.5 us (8%)
  between operations  13.3 us (4%)
  other arithmetic  9.61 us (3%)
    all_gather x2, waiting for transfers between devices, half_branch(): tokens = lax.all_gather(normed, 'tp', axis=0, tiled=True)  125 us
    reduce_scatter x2, waiting for transfers between devices, half_branch(): lax.psum_scatter(jnp.dot(hidden, down_full, preferred_element_type=jnp.fl...  108 us
    all_gather x1, waiting for transfers between devices, gather_turned(): result = lax.all_gather(both, axis, axis=0, tiled=True)  85.3 us
    dot_general x2, matrix products, half_branch(): jnp.dot(hidden, down_full, preferred_element_type=jnp.float32)  20 us
    dot_general x2, matrix products, half_branch(): gate_act = jnp.dot(tokens, gathered[0], preferred_element_type=jnp.float32)  10.4 us
  transfers between devices with their start and end apart: 5, of which 5 were waited for; matrix products, arithmetic and copies ran while one was open for 0% of the time, Pallas kernels for 0%

commit v1 on v0

v1 whole, which is shorter than its diff:
```python
import functools

import jax
import jax.numpy as jnp
from jax import lax
from jax.experimental import pallas as pl
from jax.experimental.pallas import tpu as pltpu
from jax.sharding import PartitionSpec as P

MESH = pl.DeviceIdType.MESH
F32 = jnp.float32
BF16 = jnp.bfloat16
SUBS = 4
CORES = 2


def rms_norm(rows_f, gain):
    scale = lax.rsqrt(jnp.mean(rows_f * rows_f, axis=-1, keepdims=True) + 1e-06)
    return (rows_f * scale * gain.astype(F32)).astype(BF16)


def kernel(
    n_x, n_y,
    stream, gain1, g1, u1, d1, gain2, g2, u2, d2,
    out,
    wg, wu, wd, st, x1, p1, s1, mid, x2, p2, s2, rg, ru, rd, hid, res,
    load_sem, ag1_recv, rs1_recv, ag2_recv, rs2_recv, y_recv, sib_recv, rel_recv, fin_recv,
    ag1_send, rs1_send, ag2_send, rs2_send, y_send, sib_send, rel_send, fin_send, out_sem,
):
    x = lax.axis_index("tp")
    f = lax.axis_index("fs")
    y = f // CORES
    c = f % CORES
    d = 1 - 2 * c
    hops = n_x - 1
    wide = n_x // 2
    leap = n_x // 4
    rows = st.shape[0]
    sub = rows // SUBS
    shard = g1.shape[0]
    y_hops = n_y - 1
    per_set = 3 * y_hops

    x_next = {"tp": (x + d + n_x) % n_x}
    x_prev = {"tp": (x - d + n_x) % n_x}
    x_leap = {"tp": (x + leap * d + n_x) % n_x}
    x_leap_back = {"tp": (x - leap * d + n_x) % n_x}
    y_next = {"fs": CORES * ((y + d + n_y) % n_y) + c}
    y_prev = {"fs": CORES * ((y - d + n_y) % n_y) + c}
    sibling = {"fs": CORES * y + 1 - c}

    def remote(src, dst, send, recv, device):
        return pltpu.make_async_remote_copy(
            src_ref=src, dst_ref=dst, send_sem=send, recv_sem=recv,
            device_id=device, device_id_type=MESH,
        )

    def piece(w, mat, owner):
        span = pl.ds(pl.multiple_of(owner * shard, shard), shard)
        if mat == 0:
            return wg.at[w, span, :]
        if mat == 1:
            return wu.at[w, span, :]
        return wd.at[w, :, span]

    def many(w, mat, count):
        span = pl.ds(0, count * shard)
        if mat == 0:
            return wg.at[w, span, :]
        if mat == 1:
            return wu.at[w, span, :]
        return wd.at[w, :, span]

    def tok(ref, k, m):
        return ref.at[k, pl.ds(m * sub, sub), :]

    loads = [pltpu.make_async_copy(stream, st, load_sem.at[0])]
    for i, (src, w, mat) in enumerate(
        ((g1, 0, 0), (u1, 0, 1), (d1, 0, 2), (g2, 1, 0), (u2, 1, 1), (d2, 1, 2))
    ):
        loads.append(pltpu.make_async_copy(src, piece(w, mat, f), load_sem.at[1 + i]))
    for copy in loads:
        copy.start()
    barrier = pltpu.get_barrier_semaphore()
    partners = [x_next, x_prev, y_next, y_prev, sibling]
    if leap > 1:
        partners += [x_leap, x_leap_back]
    for device in partners:
        pl.semaphore_signal(barrier, inc=1, device_id=device, device_id_type=MESH)
    pl.semaphore_wait(barrier, len(partners))

    def share(w, mat, owner):
        ref = piece(w, mat, owner)
        remote(ref, ref, sib_send.at[w * 3 + mat], sib_recv.at[w * 3 + mat], sibling).start()

    def pass_on(w, mat, owner, n):
        ref = piece(w, mat, owner)
        remote(ref, ref, y_send.at[w * 3 + mat], y_recv.at[n], y_next).start()

    def own(w, mat):
        if w == 2:
            ref = piece(2, mat, f)
            remote(ref, ref, fin_send.at[mat], fin_recv.at[mat], x_leap).wait_recv()
        pass_on(w, mat, f, w * per_set + mat)
        share(w, mat, f)

    def y_tick(n):
        w = n // per_set
        r = n % per_set
        step = r // 3
        owner = CORES * ((y - d * (step + 1) + CORES * n_y) % n_y) + c

        def arrived(mat):
            ref = piece(w, mat, owner)
            remote(ref, ref, y_send.at[w * 3 + mat], y_recv.at[n], y_next).wait_recv()

            @pl.when(step < y_hops - 1)
            def _():
                pass_on(w, mat, owner, n + 3)

            for done in range(2):
                @pl.when((step == y_hops - 1) & (w == done))
                def _():
                    own(done + 1, mat)

            share(w, mat, owner)

        for mat in range(3):
            @pl.when((n < 3 * per_set) & (r % 3 == mat))
            def _():
                arrived(mat)

    def wait_siblings(w):
        for mat in range(3):
            ref = many(w, mat, n_y)
            remote(ref, ref, sib_send.at[w * 3 + mat], sib_recv.at[w * 3 + mat], sibling).wait_recv()

    for mat in range(3):
        loads[1 + mat].wait()
        own(0, mat)

    loads[0].wait()
    for m in range(SUBS):
        part = pl.ds(m * sub, sub)
        x1[0, part, :] = rms_norm(st[part, :].astype(F32), gain1[...])
        remote(tok(x1, 0, m), tok(x1, 1, m), ag1_send, ag1_recv.at[m], x_next).start()

    relay = (rg, ru, rd)
    for mat in range(3):
        loads[4 + mat].wait()
        remote(piece(1, mat, f), relay[mat], rel_send.at[mat], rel_recv.at[mat], x_leap).start()

    def ag1_tick(k, m, last):
        remote(tok(x1, k, m), tok(x1, k, m), ag1_send, ag1_recv.at[(k - 1) * SUBS + m], x_next).wait_recv()
        if not last:
            remote(tok(x1, k, m), tok(x1, k + 1, m), ag1_send, ag1_recv.at[k * SUBS + m], x_next).start()

    relay_at = max(1, n_y // 2 - 1)

    def gather_first(k, carry):
        @pl.when(k == relay_at)
        def _():
            for mat in range(3):
                remote(relay[mat], relay[mat], rel_send.at[mat], rel_recv.at[mat], x_leap).wait_recv()
                remote(relay[mat], piece(2, mat, f), fin_send.at[mat], fin_recv.at[mat], x_leap).start()

        for m in range(SUBS):
            ag1_tick(k, m, False)
            y_tick((k - 1) * SUBS + m)
        return carry

    lax.fori_loop(1, hops, gather_first, 0)
    wait_siblings(0)

    def hidden_part(tokens, w, lo, width):
        gate = jnp.dot(tokens, wg[w, :, lo:lo + width], preferred_element_type=F32)
        up = jnp.dot(tokens, wu[w, :, lo:lo + width], preferred_element_type=F32)
        return ((gate / (1.0 + jnp.exp(-gate))) * up).astype(BF16)

    ff = wg.shape[2]
    feats = wd.shape[2]

    def first_quarter(k, m):
        if m < 2:
            width = ff // 2
            lo = m * width
            hid[0, :, lo:lo + width] = hidden_part(x1[k], 0, lo, width)
        else:
            width = feats // 2
            lo = (m - 2) * width
            p1[k, :, lo:lo + width] = jnp.dot(
                hid[0], wd[0, :, lo:lo + width], preferred_element_type=F32
            ).astype(BF16)

    def rs1_copy(src, k, m):
        return remote(src, tok(s1, k - 1, m), rs1_send, rs1_recv.at[(k - 1) * SUBS + m], x_next)

    def reduce_first(j, carry):
        for m in range(SUBS):
            @pl.when(j == 0)
            def _():
                ag1_tick(hops, m, True)

            @pl.when(j == 1)
            def _():
                rs1_copy(tok(p1, 1, m), 1, m).start()

            @pl.when(j >= 2)
            def _():
                part = pl.ds(m * sub, sub)
                rs1_copy(tok(s1, j - 2, m), j - 1, m).wait_recv()
                s1[j - 2, part, :] = (
                    s1[j - 2, part, :].astype(F32) + p1[j, part, :].astype(F32)
                ).astype(BF16)
                rs1_copy(tok(s1, j - 2, m), j, m).start()

            y_tick((hops - 1 + j) * SUBS + m)
            first_quarter((j + 1) % n_x, m)
        return carry

    lax.fori_loop(0, n_x, reduce_first, 0)

    for m in range(SUBS):
        part = pl.ds(m * sub, sub)
        rs1_copy(tok(s1, hops - 1, m), hops, m).wait_recv()
        total = s1[hops - 1, part, :].astype(F32) + p1[0, part, :].astype(F32)
        middle = (st[part, :].astype(F32) + 0.5 * total).astype(BF16)
        mid[part, :] = middle
        x2[0, part, :] = rms_norm(middle.astype(F32), gain2[...])
        remote(tok(x2, 0, m), tok(x2, 1, m), ag2_send, ag2_recv.at[m], x_next).start()
        y_tick((hops - 1 + n_x) * SUBS + m)

    def rest(n, carry):
        y_tick(n)
        return carry

    lax.fori_loop((hops + n_x) * SUBS, 3 * per_set, rest, 0)
    wait_siblings(1)
    wait_siblings(2)

    def second_quarter(k, m):
        if m < 2:
            width = ff // 2
            for lo in (0, width):
                hid[m, :, lo:lo + width] = hidden_part(x2[k], 1 + m, lo, width)
        else:
            width = feats // 2
            lo = (m - 2) * width
            p2[k, :, lo:lo + width] = (
                jnp.dot(hid[0], wd[1, :, lo:lo + width], preferred_element_type=F32)
                + jnp.dot(hid[1], wd[2, :, lo:lo + width], preferred_element_type=F32)
            ).astype(BF16)

    def gather_second(k, carry):
        for m in range(SUBS):
            @pl.when(k < wide)
            def _():
                remote(tok(x2, k, m), tok(x2, k, m), ag2_send, ag2_recv.at[(k - 1) * SUBS + m], x_next).wait_recv()

            @pl.when(k < wide - 1)
            def _():
                remote(tok(x2, k, m), tok(x2, k + 1, m), ag2_send, ag2_recv.at[k * SUBS + m], x_next).start()

            second_quarter(k - 1, m)
        return carry

    lax.fori_loop(1, wide + 1, gather_second, 0)

    def rs2_copy(src, k, m):
        return remote(src, tok(s2, k - 1, m), rs2_send, rs2_recv.at[(k - 1) * SUBS + m], x_prev)

    for m in range(SUBS):
        rs2_copy(tok(p2, wide - 1, m), wide - 1, m).start()

    for k in range(wide - 2, 0, -1):
        for m in range(SUBS):
            part = pl.ds(m * sub, sub)
            rs2_copy(tok(s2, k, m), k + 1, m).wait_recv()
            s2[k, part, :] = (
                s2[k, part, :].astype(F32) + p2[k, part, :].astype(F32)
            ).astype(BF16)
            rs2_copy(tok(s2, k, m), k, m).start()

    stores = []
    for m in range(SUBS):
        part = pl.ds(m * sub, sub)
        rs2_copy(tok(s2, 0, m), 1, m).wait_recv()
        total = s2[0, part, :].astype(F32) + p2[0, part, :].astype(F32)
        res[part, :] = (mid[part, :].astype(F32) + 0.5 * total).astype(BF16)
        copy = pltpu.make_async_copy(res.at[part, :], out.at[part, :], out_sem.at[m])
        copy.start()
        stores.append(copy)

    def sent(ref, sem):
        remote(ref, ref, sem, rel_recv.at[0], sibling).wait_send()

    sent(x1.at[pl.ds(0, hops)], ag1_send)
    sent(s1, rs1_send)
    sent(x2.at[pl.ds(0, wide - 1)], ag2_send)
    sent(s2, rs2_send)
    for mat in range(3):
        sent(relay[mat], rel_send.at[mat])
        sent(relay[mat], fin_send.at[mat])
        for w in range(3):
            sent(many(w, mat, y_hops), y_send.at[w * 3 + mat])
            sent(many(w, mat, n_y), sib_send.at[w * 3 + mat])
    for copy in stores:
        copy.wait()


def solution(mesh):
    n_x = mesh.shape["tp"]
    n_y = mesh.shape["fs"] // CORES

    def local(stream, gain1, g1, u1, d1, gain2, g2, u2, d2):
        rows, feats = stream.shape
        shard, ff = g1.shape
        wide = n_x // 2
        any_spec = pl.BlockSpec(memory_space=pl.ANY)
        vmem_spec = pl.BlockSpec(memory_space=pltpu.VMEM)
        dma = pltpu.SemaphoreType.DMA
        y_count = 9 * (n_y - 1)
        return pl.pallas_call(
            functools.partial(kernel, n_x, n_y),
            out_shape=jax.ShapeDtypeStruct((rows, feats), BF16),
            in_specs=[any_spec, vmem_spec, any_spec, any_spec, any_spec,
                      vmem_spec, any_spec, any_spec, any_spec],
            out_specs=any_spec,
            scratch_shapes=[
                pltpu.VMEM((3, feats, ff), BF16),
                pltpu.VMEM((3, feats, ff), BF16),
                pltpu.VMEM((3, ff, feats), BF16),
                pltpu.VMEM((rows, feats), BF16),
                pltpu.VMEM((n_x, rows, feats), BF16),
                pltpu.VMEM((n_x, rows, feats), BF16),
                pltpu.VMEM((n_x - 1, rows, feats), BF16),
                pltpu.VMEM((rows, feats), BF16),
                pltpu.VMEM((wide, rows, feats), BF16),
                pltpu.VMEM((wide, rows, feats), BF16),
                pltpu.VMEM((wide - 1, rows, feats), BF16),
                pltpu.VMEM((shard, ff), BF16),
                pltpu.VMEM((shard, ff), BF16),
                pltpu.VMEM((ff, shard), BF16),
                pltpu.VMEM((2, rows, ff), BF16),
                pltpu.VMEM((rows, feats), BF16),
                dma((7,)),
                dma(((n_x - 1) * SUBS,)),
                dma(((n_x - 1) * SUBS,)),
                dma(((wide - 1) * SUBS,)),
                dma(((wide - 1) * SUBS,)),
                dma((y_count,)),
                dma((9,)),
                dma((3,)),
                dma((3,)),
                dma,
                dma,
                dma,
                dma,
                dma((9,)),
                dma((9,)),
                dma((3,)),
                dma((3,)),
                dma((SUBS,)),
            ],
            compiler_params=pltpu.CompilerParams(
                collective_id=0, has_side_effects=True, vmem_limit_bytes=60 * 1024 * 1024
            ),
        )(stream, gain1.reshape(1, -1), g1, u1, d1, gain2.reshape(1, -1), g2, u2, d2)

    tokens = P(("grp", "fs", "tp"), None)
    rows_split, cols_split = P("fs", "tp"), P("tp", "fs")
    in_specs = (
        tokens,
        P(), rows_split, rows_split, cols_split,
        P(), rows_split, rows_split, cols_split,
    )
    return jax.shard_map(local, mesh=mesh, in_specs=in_specs, out_specs=tokens, check_vma=False)
```

time: 377 us -> 173 us (0.46)
  waiting for transfers between devices: 319 us -> 0 us
  Pallas kernels: 0 us -> 168 us
  matrix products: 30.5 us -> 0 us
  between operations: 13.3 us -> 0.01 us
  other arithmetic: 9.61 us -> 0 us
    all_gather x3 -> x0, waiting for transfers between devices: 210 us -> none  [the longest x2 125 us: half_branch(): tokens = lax.all_gather(normed, 'tp', axis=0, tiled=True)]
    pallas_call x0 -> x1, Pallas kernels: none -> 168 us  [local(): pl.pallas_call(functools.partial(kernel, n_x, n_y), out_shape=jax.ShapeDt...]
    reduce_scatter x2 -> x0, waiting for transfers between devices: 108 us -> none  [half_branch(): lax.psum_scatter(jnp.dot(hidden, down_full, preferred_element_type=jnp.fl...]
    dot_general x4 -> x0, matrix products: 30.5 us -> none  [the longest x2 20 us: half_branch(): jnp.dot(hidden, down_full, preferred_element_type=jnp.float32)]
    convert_element_type x5 -> x0, other arithmetic: 6.92 us -> none  [the longest x2 4.09 us: half_branch(): normed = (stream_f * lax.rsqrt(jnp.mean(stream_f * stream_f, axis=-1, kee...]
  transfers between devices with their start and end apart: 5 -> 0, of which waited for: 5 -> 0; matrix products, arithmetic and copies ran while one was open for 0% -> 0% of each run, Pallas kernels for 0% -> 0%
where the time goes in v1:
time: 173 us; the launch traced here: 171 us
  Pallas kernels  168 us (97%)
  local copies, waits for them, and re-layouts  3.79 us (2%)
    pallas_call x1, Pallas kernels, local(): pl.pallas_call(functools.partial(kernel, n_x, n_y), out_shape=jax.ShapeDt...  168 us

profile of v1, /device:TPU:514, one launch (start us, length us, event | category | flops | bytes accessed | tf_op | source)
XLA Modules:
  0.0 171.5 jit_solution(9410133577789319049)
XLA Ops:
  0.0 0.0 copy-start
  0.0 1.3 reshape.6.gain1
  1.3 0.0 copy-done
  1.3 0.6 reshape.7.gain2
  1.9 167.7 %shard_map.91 = bf16[128,2048]{1,0:T(8,128)(2,1)} custom-call(bf16[128,2048]{1,0:T(8,128)(2,1)} %stream.1, bf16[1,2048]{1,0:T(2,128)(2,1)} %reshape.6.gain1, bf16[128,512]{1,0:T(8,128)(2,1)} %g1.1, bf16[128,512]{1,0:T(8,128)(2,1)} %u1_.1, bf16[512,128]{1,0:T(8,128)(2,1)} %d1.1, bf16[1,2048]{1,0:T(2,128)(2,1)} %reshape.7.gain2, bf16[128,512]{1,0:T(8,128)(2,1)} %g2.1, ...), custom_call_target="tpu_custom_call" | custom-call | tf_op jit(solution)/shard_map/pallas_call | solution.py:323
  169.6 1.9 %copy.11 = bf16[128,2048]{1,0:T(8,128)(2,1)} copy(bf16[128,2048]{1,0:T(8,128)(2,1)} %shard_map.91) | data formatting | bytes 1048576
Async XLA Ops:
  0.0 1.3 copy-start

commit v2 on v1

--- a/solution.py
+++ b/solution.py
@@ -12,20 +12,21 @@
 BF16 = jnp.bfloat16
 SUBS = 4
 CORES = 2
+LANES = 128
 
 
 def rms_norm(rows_f, gain):
     scale = lax.rsqrt(jnp.mean(rows_f * rows_f, axis=-1, keepdims=True) + 1e-06)
-    return (rows_f * scale * gain.astype(F32)).astype(BF16)
+    return (rows_f * scale * gain).astype(BF16)
 
 
 def kernel(
     n_x, n_y,
     stream, gain1, g1, u1, d1, gain2, g2, u2, d2,
     out,
-    wg, wu, wd, st, x1, p1, s1, mid, x2, p2, s2, rg, ru, rd, hid, res,
+    wg, wu, wd, st, x1, p1, s1, mid, x2, p2, s2, rg, ru, rd, hid, gains,
     load_sem, ag1_recv, rs1_recv, ag2_recv, rs2_recv, y_recv, sib_recv, rel_recv, fin_recv,
-    ag1_send, rs1_send, ag2_send, rs2_send, y_send, sib_send, rel_send, fin_send, out_sem,
+    ag1_send, rs1_send, ag2_send, rs2_send, y_send, sib_send, rel_send, fin_send,
 ):
     x = lax.axis_index("tp")
     f = lax.axis_index("fs")
@@ -72,7 +73,7 @@
         return wd.at[w, :, span]
 
     def tok(ref, k, m):
-        return ref.at[k, pl.ds(m * sub, sub), :]
+        return ref.at[k, pl.ds(pl.multiple_of(m * sub, sub), sub), :]
 
     loads = [pltpu.make_async_copy(stream, st, load_sem.at[0])]
     for i, (src, w, mat) in enumerate(
@@ -81,6 +82,9 @@
         loads.append(pltpu.make_async_copy(src, piece(w, mat, f), load_sem.at[1 + i]))
     for copy in loads:
         copy.start()
+    for i, gain in enumerate((gain1, gain2)):
+        for j in range(gain.shape[0]):
+            gains[i, :, j * LANES:(j + 1) * LANES] = gain[j:j + 1, :].astype(F32)
     barrier = pltpu.get_barrier_semaphore()
     partners = [x_next, x_prev, y_next, y_prev, sibling]
     if leap > 1:
@@ -142,7 +146,7 @@
     loads[0].wait()
     for m in range(SUBS):
         part = pl.ds(m * sub, sub)
-        x1[0, part, :] = rms_norm(st[part, :].astype(F32), gain1[...])
+        x1[0, part, :] = rms_norm(st[part, :].astype(F32), gains[0])
         remote(tok(x1, 0, m), tok(x1, 1, m), ag1_send, ag1_recv.at[m], x_next).start()
 
     relay = (rg, ru, rd)
@@ -157,19 +161,34 @@
 
     relay_at = max(1, n_y // 2 - 1)
 
-    def gather_first(k, carry):
+    pause = 3 * leap
+
+    def extra(n, count):
+        def body(i, carry):
+            y_tick(n + i)
+            return carry
+        lax.fori_loop(0, count, body, 0)
+
+    def gather_first(k, n):
         @pl.when(k == relay_at)
         def _():
             for mat in range(3):
                 remote(relay[mat], relay[mat], rel_send.at[mat], rel_recv.at[mat], x_leap).wait_recv()
                 remote(relay[mat], piece(2, mat, f), fin_send.at[mat], fin_recv.at[mat], x_leap).start()
 
+        late = (k == 2) | (k == relay_at + 1)
+
+        @pl.when(late)
+        def _():
+            extra(n, pause)
+
+        n = n + jnp.where(late, pause, 0)
         for m in range(SUBS):
             ag1_tick(k, m, False)
-            y_tick((k - 1) * SUBS + m)
-        return carry
-
-    lax.fori_loop(1, hops, gather_first, 0)
+            y_tick(n + m)
+        return n + SUBS
+
+    ticks = lax.fori_loop(1, hops - 1, gather_first, 0)
     wait_siblings(0)
 
     def hidden_part(tokens, w, lo, width):
@@ -195,14 +214,15 @@
     def rs1_copy(src, k, m):
         return remote(src, tok(s1, k - 1, m), rs1_send, rs1_recv.at[(k - 1) * SUBS + m], x_next)
 
-    def reduce_first(j, carry):
+    def reduce_first(j, n):
         for m in range(SUBS):
             @pl.when(j == 0)
             def _():
+                ag1_tick(hops - 1, m, False)
+
+            @pl.when(j == 1)
+            def _():
                 ag1_tick(hops, m, True)
-
-            @pl.when(j == 1)
-            def _():
                 rs1_copy(tok(p1, 1, m), 1, m).start()
 
             @pl.when(j >= 2)
@@ -214,11 +234,11 @@
                 ).astype(BF16)
                 rs1_copy(tok(s1, j - 2, m), j, m).start()
 
-            y_tick((hops - 1 + j) * SUBS + m)
+            y_tick(n + m)
             first_quarter((j + 1) % n_x, m)
-        return carry
-
-    lax.fori_loop(0, n_x, reduce_first, 0)
+        return n + SUBS
+
+    ticks = lax.fori_loop(0, n_x, reduce_first, ticks)
 
     for m in range(SUBS):
         part = pl.ds(m * sub, sub)
@@ -226,51 +246,63 @@
         total = s1[hops - 1, part, :].astype(F32) + p1[0, part, :].astype(F32)
         middle = (st[part, :].astype(F32) + 0.5 * total).astype(BF16)
         mid[part, :] = middle
-        x2[0, part, :] = rms_norm(middle.astype(F32), gain2[...])
+        x2[0, part, :] = rms_norm(middle.astype(F32), gains[1])
         remote(tok(x2, 0, m), tok(x2, 1, m), ag2_send, ag2_recv.at[m], x_next).start()
-        y_tick((hops - 1 + n_x) * SUBS + m)
 
     def rest(n, carry):
         y_tick(n)
         return carry
 
-    lax.fori_loop((hops + n_x) * SUBS, 3 * per_set, rest, 0)
+    lax.fori_loop(ticks, 3 * per_set, rest, 0)
     wait_siblings(1)
     wait_siblings(2)
 
-    def second_quarter(k, m):
+    def second_quarter(k, m, lo_row, count):
+        tokens = pl.ds(lo_row, count)
         if m < 2:
             width = ff // 2
             for lo in (0, width):
-                hid[m, :, lo:lo + width] = hidden_part(x2[k], 1 + m, lo, width)
+                hid[m, tokens, lo:lo + width] = hidden_part(x2[k, tokens, :], 1 + m, lo, width)
         else:
             width = feats // 2
             lo = (m - 2) * width
-            p2[k, :, lo:lo + width] = (
-                jnp.dot(hid[0], wd[1, :, lo:lo + width], preferred_element_type=F32)
-                + jnp.dot(hid[1], wd[2, :, lo:lo + width], preferred_element_type=F32)
+            p2[k, tokens, lo:lo + width] = (
+                jnp.dot(hid[0, tokens, :], wd[1, :, lo:lo + width], preferred_element_type=F32)
+                + jnp.dot(hid[1, tokens, :], wd[2, :, lo:lo + width], preferred_element_type=F32)
             ).astype(BF16)
+
+    def ag2_arrival(k, m):
+        remote(tok(x2, k, m), tok(x2, k, m), ag2_send, ag2_recv.at[(k - 1) * SUBS + m], x_next).wait_recv()
 
     def gather_second(k, carry):
         for m in range(SUBS):
-            @pl.when(k < wide)
-            def _():
-                remote(tok(x2, k, m), tok(x2, k, m), ag2_send, ag2_recv.at[(k - 1) * SUBS + m], x_next).wait_recv()
-
             @pl.when(k < wide - 1)
             def _():
+                ag2_arrival(k, m)
                 remote(tok(x2, k, m), tok(x2, k + 1, m), ag2_send, ag2_recv.at[k * SUBS + m], x_next).start()
 
-            second_quarter(k - 1, m)
+            if m < 2:
+                second_quarter(k - 1, 2 * m, 0, rows)
+                second_quarter(k - 1, 2 * m + 1, 0, rows)
         return carry
 
-    lax.fori_loop(1, wide + 1, gather_second, 0)
+    lax.fori_loop(1, wide, gather_second, 0)
 
     def rs2_copy(src, k, m):
         return remote(src, tok(s2, k - 1, m), rs2_send, rs2_recv.at[(k - 1) * SUBS + m], x_prev)
 
-    for m in range(SUBS):
-        rs2_copy(tok(p2, wide - 1, m), wide - 1, m).start()
+    half = rows // 2
+
+    def last_block(h, carry):
+        for m in range(SUBS // 2):
+            ag2_arrival(wide - 1, h * (SUBS // 2) + m)
+        for q in range(4):
+            second_quarter(wide - 1, q, pl.multiple_of(h * half, half), half)
+        for m in range(SUBS // 2):
+            rs2_copy(tok(p2, wide - 1, h * (SUBS // 2) + m), wide - 1, h * (SUBS // 2) + m).start()
+        return carry
+
+    lax.fori_loop(0, 2, last_block, 0)
 
     for k in range(wide - 2, 0, -1):
         for m in range(SUBS):
@@ -281,15 +313,11 @@
             ).astype(BF16)
             rs2_copy(tok(s2, k, m), k, m).start()
 
-    stores = []
     for m in range(SUBS):
         part = pl.ds(m * sub, sub)
         rs2_copy(tok(s2, 0, m), 1, m).wait_recv()
         total = s2[0, part, :].astype(F32) + p2[0, part, :].astype(F32)
-        res[part, :] = (mid[part, :].astype(F32) + 0.5 * total).astype(BF16)
-        copy = pltpu.make_async_copy(res.at[part, :], out.at[part, :], out_sem.at[m])
-        copy.start()
-        stores.append(copy)
+        out[part, :] = (mid[part, :].astype(F32) + 0.5 * total).astype(BF16)
 
     def sent(ref, sem):
         remote(ref, ref, sem, rel_recv.at[0], sibling).wait_send()
@@ -304,8 +332,6 @@
         for w in range(3):
             sent(many(w, mat, y_hops), y_send.at[w * 3 + mat])
             sent(many(w, mat, n_y), sib_send.at[w * 3 + mat])
-    for copy in stores:
-        copy.wait()
 
 
 def solution(mesh):
@@ -325,7 +351,7 @@
             out_shape=jax.ShapeDtypeStruct((rows, feats), BF16),
             in_specs=[any_spec, vmem_spec, any_spec, any_spec, any_spec,
                       vmem_spec, any_spec, any_spec, any_spec],
-            out_specs=any_spec,
+            out_specs=vmem_spec,
             scratch_shapes=[
                 pltpu.VMEM((3, feats, ff), BF16),
                 pltpu.VMEM((3, feats, ff), BF16),
@@ -342,7 +368,7 @@
                 pltpu.VMEM((shard, ff), BF16),
                 pltpu.VMEM((ff, shard), BF16),
                 pltpu.VMEM((2, rows, ff), BF16),
-                pltpu.VMEM((rows, feats), BF16),
+                pltpu.VMEM((2, 1, feats), F32),
                 dma((7,)),
                 dma(((n_x - 1) * SUBS,)),
                 dma(((n_x - 1) * SUBS,)),
@@ -360,12 +386,11 @@
                 dma((9,)),
                 dma((3,)),
                 dma((3,)),
-                dma((SUBS,)),
             ],
             compiler_params=pltpu.CompilerParams(
                 collective_id=0, has_side_effects=True, vmem_limit_bytes=60 * 1024 * 1024
             ),
-        )(stream, gain1.reshape(1, -1), g1, u1, d1, gain2.reshape(1, -1), g2, u2, d2)
+        )(stream, gain1.reshape(-1, LANES), g1, u1, d1, gain2.reshape(-1, LANES), g2, u2, d2)
 
     tokens = P(("grp", "fs", "tp"), None)
     rows_split, cols_split = P("fs", "tp"), P("tp", "fs")

time: 173 us -> 169 us (0.977)
  Pallas kernels: 168 us -> 166 us
  local copies, waits for them, and re-layouts: 3.79 us -> 1.88 us
    reshape x2 -> x0, local copies, waits for them, and re-layouts: 1.9 us -> none  [the longest x1 1.3 us: local(): gain1.reshape(1, -1)]
    pallas_call x1, Pallas kernels: 168 us -> 166 us  [local(): pl.pallas_call(functools.partial(kernel, n_x, n_y), out_shape=jax.ShapeDt...]
where the time goes in v2:
time: 169 us; the launch traced here: 168 us
  Pallas kernels  166 us (98%)
  local copies, waits for them, and re-layouts  1.88 us (1%)
    pallas_call x1, Pallas kernels, local(): pl.pallas_call(functools.partial(kernel, n_x, n_y), out_shape=jax.ShapeDt...  166 us

profile of v2, /device:TPU:514, one launch (start us, length us, event | category | flops | bytes accessed | tf_op | source)
XLA Modules:
  0.0 167.8 jit_solution(215140585630041001)
XLA Ops:
  0.0 165.9 %shard_map.91 = bf16[128,2048]{1,0:T(8,128)(2,1)} custom-call(bf16[128,2048]{1,0:T(8,128)(2,1)} %stream.1, bf16[16,128]{1,0:T(8,128)(2,1)} %bitcast.2, bf16[128,512]{1,0:T(8,128)(2,1)} %g1.1, bf16[128,512]{1,0:T(8,128)(2,1)} %u1_.1, bf16[512,128]{1,0:T(8,128)(2,1)} %d1.1, bf16[16,128]{1,0:T(8,128)(2,1)} %bitcast.3, bf16[128,512]{1,0:T(8,128)(2,1)} %g2.1, ...), custom_call_target="tpu_custom_call" | custom-call | tf_op jit(solution)/shard_map/pallas_call | solution.py:349
  165.9 1.9 %copy.11 = bf16[128,2048]{1,0:T(8,128)(2,1)} copy(bf16[128,2048]{1,0:T(8,128)(2,1)} %shard_map.91) | data formatting | bytes 1048576

commit v3 on v2

--- a/solution.py
+++ b/solution.py
@@ -26,7 +26,7 @@
     out,
     wg, wu, wd, st, x1, p1, s1, mid, x2, p2, s2, rg, ru, rd, hid, gains,
     load_sem, ag1_recv, rs1_recv, ag2_recv, rs2_recv, y_recv, sib_recv, rel_recv, fin_recv,
-    ag1_send, rs1_send, ag2_send, rs2_send, y_send, sib_send, rel_send, fin_send,
+    ag1_send, rs1_send, ag2_send, rs2_send, y_send, sib_send, rel_send, fin_send, turn,
 ):
     x = lax.axis_index("tp")
     f = lax.axis_index("fs")
@@ -75,6 +75,12 @@
     def tok(ref, k, m):
         return ref.at[k, pl.ds(pl.multiple_of(m * sub, sub), sub), :]
 
+    barrier = pltpu.get_barrier_semaphore()
+    partners = [x_next, x_prev, y_next, y_prev, sibling]
+    if leap > 1:
+        partners += [x_leap, x_leap_back]
+    for device in partners:
+        pl.semaphore_signal(barrier, inc=1, device_id=device, device_id_type=MESH)
     loads = [pltpu.make_async_copy(stream, st, load_sem.at[0])]
     for i, (src, w, mat) in enumerate(
         ((g1, 0, 0), (u1, 0, 1), (d1, 0, 2), (g2, 1, 0), (u2, 1, 1), (d2, 1, 2))
@@ -85,12 +91,6 @@
     for i, gain in enumerate((gain1, gain2)):
         for j in range(gain.shape[0]):
             gains[i, :, j * LANES:(j + 1) * LANES] = gain[j:j + 1, :].astype(F32)
-    barrier = pltpu.get_barrier_semaphore()
-    partners = [x_next, x_prev, y_next, y_prev, sibling]
-    if leap > 1:
-        partners += [x_leap, x_leap_back]
-    for device in partners:
-        pl.semaphore_signal(barrier, inc=1, device_id=device, device_id_type=MESH)
     pl.semaphore_wait(barrier, len(partners))
 
     def share(w, mat, owner):
@@ -161,7 +161,7 @@
 
     relay_at = max(1, n_y // 2 - 1)
 
-    pause = 3 * leap
+    pause = 3 * leap - 1
 
     def extra(n, count):
         def body(i, carry):
@@ -185,10 +185,19 @@
         n = n + jnp.where(late, pause, 0)
         for m in range(SUBS):
             ag1_tick(k, m, False)
-            y_tick(n + m)
-        return n + SUBS
+
+            @pl.when(k > 1)
+            def _():
+                y_tick(n + m)
+        return n + jnp.where(k > 1, SUBS, 0)
+
+    def rest(n, carry):
+        y_tick(n)
+        return carry
 
     ticks = lax.fori_loop(1, hops - 1, gather_first, 0)
+    lax.fori_loop(ticks, per_set, rest, 0)
+    ticks = jnp.maximum(ticks, per_set)
     wait_siblings(0)
 
     def hidden_part(tokens, w, lo, width):
@@ -248,12 +257,34 @@
         mid[part, :] = middle
         x2[0, part, :] = rms_norm(middle.astype(F32), gains[1])
         remote(tok(x2, 0, m), tok(x2, 1, m), ag2_send, ag2_recv.at[m], x_next).start()
-
-    def rest(n, carry):
-        y_tick(n)
-        return carry
-
-    lax.fori_loop(ticks, 3 * per_set, rest, 0)
+        y_tick(ticks + m)
+
+    def ag2_arrival(t):
+        k, m = 1 + t // SUBS, t % SUBS
+        remote(tok(x2, k, m), tok(x2, k, m), ag2_send, ag2_recv.at[t], x_next).wait_recv()
+
+    passes = (wide - 2) * SUBS
+
+    def hand_over():
+        pl.semaphore_signal(turn, inc=1, device_id=sibling, device_id_type=MESH)
+
+    def ag2_tick(t):
+        @pl.when(t < passes)
+        def _():
+            ag2_arrival(t)
+            k, m = 1 + t // SUBS, t % SUBS
+            remote(tok(x2, k, m), tok(x2, k + 1, m), ag2_send, ag2_recv.at[t + SUBS], x_next).start()
+
+        @pl.when(t == passes - 1)
+        def _():
+            hand_over()
+
+    for t in range(SUBS):
+        ag2_tick(t)
+    if not passes:
+        hand_over()
+
+    lax.fori_loop(ticks + SUBS, 3 * per_set, rest, 0)
     wait_siblings(1)
     wait_siblings(2)
 
@@ -271,22 +302,14 @@
                 + jnp.dot(hid[1, tokens, :], wd[2, :, lo:lo + width], preferred_element_type=F32)
             ).astype(BF16)
 
-    def ag2_arrival(k, m):
-        remote(tok(x2, k, m), tok(x2, k, m), ag2_send, ag2_recv.at[(k - 1) * SUBS + m], x_next).wait_recv()
-
     def gather_second(k, carry):
-        for m in range(SUBS):
-            @pl.when(k < wide - 1)
-            def _():
-                ag2_arrival(k, m)
-                remote(tok(x2, k, m), tok(x2, k + 1, m), ag2_send, ag2_recv.at[k * SUBS + m], x_next).start()
-
-            if m < 2:
-                second_quarter(k - 1, 2 * m, 0, rows)
-                second_quarter(k - 1, 2 * m + 1, 0, rows)
+        for m in range(2):
+            ag2_tick(SUBS + 2 * k + m)
+            second_quarter(k, 2 * m, 0, rows)
+            second_quarter(k, 2 * m + 1, 0, rows)
         return carry
 
-    lax.fori_loop(1, wide, gather_second, 0)
+    lax.fori_loop(0, wide - 1, gather_second, 0)
 
     def rs2_copy(src, k, m):
         return remote(src, tok(s2, k - 1, m), rs2_send, rs2_recv.at[(k - 1) * SUBS + m], x_prev)
@@ -295,9 +318,14 @@
 
     def last_block(h, carry):
         for m in range(SUBS // 2):
-            ag2_arrival(wide - 1, h * (SUBS // 2) + m)
+            ag2_arrival(passes + h * (SUBS // 2) + m)
         for q in range(4):
             second_quarter(wide - 1, q, pl.multiple_of(h * half, half), half)
+
+        @pl.when(h == 0)
+        def _():
+            pl.semaphore_wait(turn, 1)
+
         for m in range(SUBS // 2):
             rs2_copy(tok(p2, wide - 1, h * (SUBS // 2) + m), wide - 1, h * (SUBS // 2) + m).start()
         return carry
@@ -348,7 +376,7 @@
         y_count = 9 * (n_y - 1)
         return pl.pallas_call(
             functools.partial(kernel, n_x, n_y),
-            out_shape=jax.ShapeDtypeStruct((rows, feats), BF16),
+            out_shape=pltpu.VMEM((rows, feats), BF16),
             in_specs=[any_spec, vmem_spec, any_spec, any_spec, any_spec,
                       vmem_spec, any_spec, any_spec, any_spec],
             out_specs=vmem_spec,
@@ -386,6 +414,7 @@
                 dma((9,)),
                 dma((3,)),
                 dma((3,)),
+                pltpu.SemaphoreType.REGULAR,
             ],
             compiler_params=pltpu.CompilerParams(
                 collective_id=0, has_side_effects=True, vmem_limit_bytes=60 * 1024 * 1024

time: 169 us -> 159 us (0.941)
  Pallas kernels: 166 us -> 158 us
    pallas_call x1, Pallas kernels: 166 us -> 158 us  [local(): pl.pallas_call(functools.partial(kernel, n_x, n_y), out_shape=pltpu.VMEM(...]
where the time goes in v3:
time: 159 us; the launch traced here: 158 us
  Pallas kernels  158 us (99%)
    pallas_call x1, Pallas kernels, local(): pl.pallas_call(functools.partial(kernel, n_x, n_y), out_shape=pltpu.VMEM(...  158 us

profile of v3, /device:TPU:514, one launch (start us, length us, event | category | flops | bytes accessed | tf_op | source)
XLA Modules:
  0.0 158.5 jit_solution(16828596708129965947)
XLA Ops:
  0.0 157.7 %shard_map.91 = bf16[128,2048]{1,0:T(8,128)(2,1)S(1)} custom-call(bf16[128,2048]{1,0:T(8,128)(2,1)} %stream.1, bf16[16,128]{1,0:T(8,128)(2,1)} %bitcast.2, bf16[128,512]{1,0:T(8,128)(2,1)} %g1.1, bf16[128,512]{1,0:T(8,128)(2,1)} %u1_.1, bf16[512,128]{1,0:T(8,128)(2,1)} %d1.1, bf16[16,128]{1,0:T(8,128)(2,1)} %bitcast.3, bf16[128,512]{1,0:T(8,128)(2,1)} %g2.1, ...), custom_call_target="tpu_custom_call" | custom-call | tf_op jit(solution)/shard_map/pallas_call | solution.py:377
  157.7 0.8 copy.11

commit v4 on v3

--- a/solution.py
+++ b/solution.py
@@ -26,7 +26,7 @@
     out,
     wg, wu, wd, st, x1, p1, s1, mid, x2, p2, s2, rg, ru, rd, hid, gains,
     load_sem, ag1_recv, rs1_recv, ag2_recv, rs2_recv, y_recv, sib_recv, rel_recv, fin_recv,
-    ag1_send, rs1_send, ag2_send, rs2_send, y_send, sib_send, rel_send, fin_send, turn,
+    ag1_send, rs1_send, ag2_send, rs2_send, y_send, sib_send, rel_send, fin_send, both_in,
 ):
     x = lax.axis_index("tp")
     f = lax.axis_index("fs")
@@ -40,10 +40,8 @@
     sub = rows // SUBS
     shard = g1.shape[0]
     y_hops = n_y - 1
-    per_set = 3 * y_hops
-
-    x_next = {"tp": (x + d + n_x) % n_x}
-    x_prev = {"tp": (x - d + n_x) % n_x}
+
+    x_near = ({"tp": (x + 1) % n_x}, {"tp": (x - 1 + n_x) % n_x})
     x_leap = {"tp": (x + leap * d + n_x) % n_x}
     x_leap_back = {"tp": (x - leap * d + n_x) % n_x}
     y_next = {"fs": CORES * ((y + d + n_y) % n_y) + c}
@@ -72,15 +70,42 @@
             return wu.at[w, span, :]
         return wd.at[w, :, span]
 
-    def tok(ref, k, m):
-        return ref.at[k, pl.ds(pl.multiple_of(m * sub, sub), sub), :]
+    bit = sub // 2
+
+    class Halves:
+        def __init__(self, src, src_k, dst, dst_k, m, send, recv, slot, back=False):
+            self.args = src, src_k, dst, dst_k, m, send, recv, slot, back
+
+        def start(self):
+            src, src_k, dst, dst_k, m, send, recv, slot, back = self.args
+            for way in range(2):
+                span = pl.ds(pl.multiple_of(m * sub, sub) + way * bit, bit)
+                remote(
+                    src.at[src_k, span, :], dst.at[dst_k, span, :], send,
+                    recv.at[slot], x_near[1 - way if back else way],
+                ).start()
+
+        def wait_recv(self):
+            _, _, dst, dst_k, m, send, recv, slot, _ = self.args
+            whole = dst.at[dst_k, pl.ds(pl.multiple_of(m * sub, sub), sub), :]
+            remote(whole, whole, send, recv.at[slot], x_near[0]).wait_recv()
+
+    def relay_on(came, goes):
+        came.wait_recv()
+        goes.start()
 
     barrier = pltpu.get_barrier_semaphore()
-    partners = [x_next, x_prev, y_next, y_prev, sibling]
+    partners = [x_near[0], x_near[1], y_next, y_prev]
     if leap > 1:
         partners += [x_leap, x_leap_back]
     for device in partners:
         pl.semaphore_signal(barrier, inc=1, device_id=device, device_id_type=MESH)
+
+    @pl.when(c == 1)
+    def _():
+        witness = {"fs": CORES * y, "tp": (x + 1) % n_x}
+        pl.semaphore_signal(barrier, inc=1, device_id=witness, device_id_type=MESH)
+
     loads = [pltpu.make_async_copy(stream, st, load_sem.at[0])]
     for i, (src, w, mat) in enumerate(
         ((g1, 0, 0), (u1, 0, 1), (d1, 0, 2), (g2, 1, 0), (u2, 1, 1), (d2, 1, 2))
@@ -91,81 +116,117 @@
     for i, gain in enumerate((gain1, gain2)):
         for j in range(gain.shape[0]):
             gains[i, :, j * LANES:(j + 1) * LANES] = gain[j:j + 1, :].astype(F32)
-    pl.semaphore_wait(barrier, len(partners))
+    pl.semaphore_wait(barrier, len(partners) + 1 - c)
+
+    @pl.when(c == 0)
+    def _():
+        for core in range(CORES):
+            device = {"fs": CORES * y + core, "tp": (x - 1 + n_x) % n_x}
+            pl.semaphore_signal(both_in, inc=1, device_id=device, device_id_type=MESH)
+
+    head = 4
+    first_ticks = head * y_hops
+    all_ticks = 9 * y_hops
 
     def share(w, mat, owner):
         ref = piece(w, mat, owner)
-        remote(ref, ref, sib_send.at[w * 3 + mat], sib_recv.at[w * 3 + mat], sibling).start()
+        remote(ref, ref, sib_send.at[mat], sib_recv.at[w * 3 + mat], sibling).start()
 
     def pass_on(w, mat, owner, n):
         ref = piece(w, mat, owner)
-        remote(ref, ref, y_send.at[w * 3 + mat], y_recv.at[n], y_next).start()
-
-    def own(w, mat):
+        remote(ref, ref, y_send.at[mat], y_recv.at[n], y_next).start()
+
+    def share_item(i):
+        owner = CORES * ((y - d * (i // head) + CORES * n_y) % n_y) + c
+        item = i % head
+        for mat in range(3):
+            @pl.when(item % 3 == mat)
+            def _():
+                share(item // 3, mat, owner)
+
+    def own(item):
+        w, mat = item // 3, item % 3
         if w == 2:
             ref = piece(2, mat, f)
             remote(ref, ref, fin_send.at[mat], fin_recv.at[mat], x_leap).wait_recv()
-        pass_on(w, mat, f, w * per_set + mat)
-        share(w, mat, f)
-
-    def y_tick(n):
-        w = n // per_set
-        r = n % per_set
-        step = r // 3
+        if item < head:
+            pass_on(w, mat, f, item)
+        else:
+            pass_on(w, mat, f, first_ticks + item - head)
+            share(w, mat, f)
+
+    def y_tick(n, sharing=True):
+        late = n >= first_ticks
+        r = n - jnp.where(late, first_ticks, 0)
+        step = jnp.where(late, r // (9 - head), r // head)
+        size = jnp.where(late, 9 - head, head)
+        item = r - step * size + jnp.where(late, head, 0)
+        w = item // 3
         owner = CORES * ((y - d * (step + 1) + CORES * n_y) % n_y) + c
 
         def arrived(mat):
             ref = piece(w, mat, owner)
-            remote(ref, ref, y_send.at[w * 3 + mat], y_recv.at[n], y_next).wait_recv()
+            remote(ref, ref, y_send.at[mat], y_recv.at[n], y_next).wait_recv()
 
             @pl.when(step < y_hops - 1)
             def _():
-                pass_on(w, mat, owner, n + 3)
-
-            for done in range(2):
-                @pl.when((step == y_hops - 1) & (w == done))
+                pass_on(w, mat, owner, n + size)
+
+            if sharing is True:
+                share(w, mat, owner)
+            else:
+                @pl.when(sharing)
                 def _():
-                    own(done + 1, mat)
-
-            share(w, mat, owner)
+                    share(w, mat, owner)
 
         for mat in range(3):
-            @pl.when((n < 3 * per_set) & (r % 3 == mat))
+            @pl.when((n < all_ticks) & (item % 3 == mat))
             def _():
                 arrived(mat)
+
+        for item_own in range(head, 9):
+            @pl.when((n < first_ticks) & (step == y_hops - 1) & (item == min(item_own - head, head - 1)))
+            def _():
+                own(item_own)
 
     def wait_siblings(w):
         for mat in range(3):
             ref = many(w, mat, n_y)
-            remote(ref, ref, sib_send.at[w * 3 + mat], sib_recv.at[w * 3 + mat], sibling).wait_recv()
-
-    for mat in range(3):
-        loads[1 + mat].wait()
-        own(0, mat)
+            remote(ref, ref, sib_send.at[mat], sib_recv.at[w * 3 + mat], sibling).wait_recv()
+
+    def ag1_copy(k, m):
+        return Halves(x1, k, x1, k + 1, m, ag1_send, ag1_recv, k * SUBS + m)
 
     loads[0].wait()
     for m in range(SUBS):
         part = pl.ds(m * sub, sub)
         x1[0, part, :] = rms_norm(st[part, :].astype(F32), gains[0])
-        remote(tok(x1, 0, m), tok(x1, 1, m), ag1_send, ag1_recv.at[m], x_next).start()
+        ag1_copy(0, m).start()
+        if m == 0:
+            for item in range(head):
+                loads[1 + item].wait()
+                own(item)
 
     relay = (rg, ru, rd)
     for mat in range(3):
-        loads[4 + mat].wait()
+        if mat:
+            loads[4 + mat].wait()
         remote(piece(1, mat, f), relay[mat], rel_send.at[mat], rel_recv.at[mat], x_leap).start()
 
     def ag1_tick(k, m, last):
-        remote(tok(x1, k, m), tok(x1, k, m), ag1_send, ag1_recv.at[(k - 1) * SUBS + m], x_next).wait_recv()
-        if not last:
-            remote(tok(x1, k, m), tok(x1, k + 1, m), ag1_send, ag1_recv.at[k * SUBS + m], x_next).start()
+        if last:
+            ag1_copy(k - 1, m).wait_recv()
+        else:
+            relay_on(ag1_copy(k - 1, m), ag1_copy(k, m))
 
     relay_at = max(1, n_y // 2 - 1)
-
-    pause = 3 * leap - 1
-
-    def extra(n, count):
+    share_at = max(1, min(relay_at + 1, hops - 2))
+
+    pause = 3 * leap
+
+    def extra(n, count, sharing):
         def body(i, carry):
-            y_tick(n + i)
+            y_tick(n + i, sharing)
             return carry
         lax.fori_loop(0, count, body, 0)
 
@@ -176,28 +237,37 @@
                 remote(relay[mat], relay[mat], rel_send.at[mat], rel_recv.at[mat], x_leap).wait_recv()
                 remote(relay[mat], piece(2, mat, f), fin_send.at[mat], fin_recv.at[mat], x_leap).start()
 
+        @pl.when(k == share_at)
+        def _():
+            pl.semaphore_wait(both_in, 1)
+
+            def body(i, carry):
+                share_item(i)
+                return carry
+            lax.fori_loop(0, jnp.maximum(n, 0) + head, body, 0)
+
         late = (k == 2) | (k == relay_at + 1)
 
         @pl.when(late)
         def _():
-            extra(n, pause)
+            extra(n, pause, k >= share_at)
 
         n = n + jnp.where(late, pause, 0)
         for m in range(SUBS):
             ag1_tick(k, m, False)
 
-            @pl.when(k > 1)
-            def _():
-                y_tick(n + m)
-        return n + jnp.where(k > 1, SUBS, 0)
+            @pl.when((k > 1) | (m >= SUBS // 2))
+            def _():
+                y_tick(n + m, k >= share_at)
+        return n + SUBS
 
     def rest(n, carry):
         y_tick(n)
         return carry
 
-    ticks = lax.fori_loop(1, hops - 1, gather_first, 0)
-    lax.fori_loop(ticks, per_set, rest, 0)
-    ticks = jnp.maximum(ticks, per_set)
+    ticks = lax.fori_loop(1, hops - 1, gather_first, -(SUBS // 2))
+    lax.fori_loop(ticks, first_ticks, rest, 0)
+    ticks = jnp.maximum(ticks, first_ticks)
     wait_siblings(0)
 
     def hidden_part(tokens, w, lo, width):
@@ -220,8 +290,8 @@
                 hid[0], wd[0, :, lo:lo + width], preferred_element_type=F32
             ).astype(BF16)
 
-    def rs1_copy(src, k, m):
-        return remote(src, tok(s1, k - 1, m), rs1_send, rs1_recv.at[(k - 1) * SUBS + m], x_next)
+    def rs1_copy(src, src_k, k, m):
+        return Halves(src, src_k, s1, k - 1, m, rs1_send, rs1_recv, (k - 1) * SUBS + m)
 
     def reduce_first(j, n):
         for m in range(SUBS):
@@ -232,16 +302,16 @@
             @pl.when(j == 1)
             def _():
                 ag1_tick(hops, m, True)
-                rs1_copy(tok(p1, 1, m), 1, m).start()
+                rs1_copy(p1, 1, 1, m).start()
 
             @pl.when(j >= 2)
             def _():
                 part = pl.ds(m * sub, sub)
-                rs1_copy(tok(s1, j - 2, m), j - 1, m).wait_recv()
+                rs1_copy(s1, j - 2, j - 1, m).wait_recv()
                 s1[j - 2, part, :] = (
                     s1[j - 2, part, :].astype(F32) + p1[j, part, :].astype(F32)
                 ).astype(BF16)
-                rs1_copy(tok(s1, j - 2, m), j, m).start()
+                rs1_copy(s1, j - 2, j, m).start()
 
             y_tick(n + m)
             first_quarter((j + 1) % n_x, m)
@@ -249,42 +319,31 @@
 
     ticks = lax.fori_loop(0, n_x, reduce_first, ticks)
 
+    def ag2_copy(t):
+        k, m = t // SUBS, t % SUBS
+        return Halves(x2, k, x2, k + 1, m, ag2_send, ag2_recv, t)
+
     for m in range(SUBS):
         part = pl.ds(m * sub, sub)
-        rs1_copy(tok(s1, hops - 1, m), hops, m).wait_recv()
+        rs1_copy(s1, hops - 1, hops, m).wait_recv()
         total = s1[hops - 1, part, :].astype(F32) + p1[0, part, :].astype(F32)
         middle = (st[part, :].astype(F32) + 0.5 * total).astype(BF16)
         mid[part, :] = middle
         x2[0, part, :] = rms_norm(middle.astype(F32), gains[1])
-        remote(tok(x2, 0, m), tok(x2, 1, m), ag2_send, ag2_recv.at[m], x_next).start()
+        ag2_copy(m).start()
         y_tick(ticks + m)
 
-    def ag2_arrival(t):
-        k, m = 1 + t // SUBS, t % SUBS
-        remote(tok(x2, k, m), tok(x2, k, m), ag2_send, ag2_recv.at[t], x_next).wait_recv()
-
     passes = (wide - 2) * SUBS
-
-    def hand_over():
-        pl.semaphore_signal(turn, inc=1, device_id=sibling, device_id_type=MESH)
 
     def ag2_tick(t):
         @pl.when(t < passes)
         def _():
-            ag2_arrival(t)
-            k, m = 1 + t // SUBS, t % SUBS
-            remote(tok(x2, k, m), tok(x2, k + 1, m), ag2_send, ag2_recv.at[t + SUBS], x_next).start()
-
-        @pl.when(t == passes - 1)
-        def _():
-            hand_over()
+            relay_on(ag2_copy(t), ag2_copy(t + SUBS))
 
     for t in range(SUBS):
         ag2_tick(t)
-    if not passes:
-        hand_over()
-
-    lax.fori_loop(ticks + SUBS, 3 * per_set, rest, 0)
+
+    lax.fori_loop(ticks + SUBS, all_ticks, rest, 0)
     wait_siblings(1)
     wait_siblings(2)
 
@@ -302,64 +361,64 @@
                 + jnp.dot(hid[1, tokens, :], wd[2, :, lo:lo + width], preferred_element_type=F32)
             ).astype(BF16)
 
-    def gather_second(k, carry):
-        for m in range(2):
-            ag2_tick(SUBS + 2 * k + m)
-            second_quarter(k, 2 * m, 0, rows)
-            second_quarter(k, 2 * m + 1, 0, rows)
-        return carry
-
-    lax.fori_loop(0, wide - 1, gather_second, 0)
+    for t in range(SUBS, passes):
+        ag2_tick(t)
+    for q in range(4 if wide > 2 else 0):
+        second_quarter(wide - 2, q, 0, rows)
 
     def rs2_copy(src, k, m):
-        return remote(src, tok(s2, k - 1, m), rs2_send, rs2_recv.at[(k - 1) * SUBS + m], x_prev)
+        return Halves(src, k, s2, k - 1, m, rs2_send, rs2_recv, (k - 1) * SUBS + m, back=True)
 
     half = rows // 2
 
     def last_block(h, carry):
         for m in range(SUBS // 2):
-            ag2_arrival(passes + h * (SUBS // 2) + m)
+            ag2_copy(passes + h * (SUBS // 2) + m).wait_recv()
         for q in range(4):
             second_quarter(wide - 1, q, pl.multiple_of(h * half, half), half)
-
-        @pl.when(h == 0)
-        def _():
-            pl.semaphore_wait(turn, 1)
-
         for m in range(SUBS // 2):
-            rs2_copy(tok(p2, wide - 1, h * (SUBS // 2) + m), wide - 1, h * (SUBS // 2) + m).start()
+            rs2_copy(p2, wide - 1, h * (SUBS // 2) + m).start()
         return carry
 
     lax.fori_loop(0, 2, last_block, 0)
 
-    for k in range(wide - 2, 0, -1):
+    def sent(ref, sem):
+        remote(ref, ref, sem, rel_recv.at[0], sibling).wait_send()
+
+    sent(x1.at[pl.ds(0, hops)], ag1_send)
+    sent(s1, rs1_send)
+    sent(x2.at[pl.ds(0, wide - 1)], ag2_send)
+    for mat in range(3):
+        sent(relay[mat], rel_send.at[mat])
+        sent(relay[mat], fin_send.at[mat])
+        sent(many(pl.ds(0, 3), mat, y_hops), y_send.at[mat])
+        sent(many(pl.ds(0, 3), mat, n_y), sib_send.at[mat])
+
+    def reduce_second(i, carry):
+        k = wide - 2 - i
         for m in range(SUBS):
             part = pl.ds(m * sub, sub)
-            rs2_copy(tok(s2, k, m), k + 1, m).wait_recv()
+            rs2_copy(s2, k + 1, m).wait_recv()
             s2[k, part, :] = (
                 s2[k, part, :].astype(F32) + p2[k, part, :].astype(F32)
             ).astype(BF16)
-            rs2_copy(tok(s2, k, m), k, m).start()
+            rs2_copy(s2, k, m).start()
+            second_quarter(k - 1, m, 0, rows)
+        return carry
+
+    if wide > 2:
+        lax.fori_loop(0, wide - 2, reduce_second, 0)
+    else:
+        for q in range(4):
+            second_quarter(0, q, 0, rows)
 
     for m in range(SUBS):
         part = pl.ds(m * sub, sub)
-        rs2_copy(tok(s2, 0, m), 1, m).wait_recv()
+        rs2_copy(s2, 1, m).wait_recv()
         total = s2[0, part, :].astype(F32) + p2[0, part, :].astype(F32)
         out[part, :] = (mid[part, :].astype(F32) + 0.5 * total).astype(BF16)
 
-    def sent(ref, sem):
-        remote(ref, ref, sem, rel_recv.at[0], sibling).wait_send()
-
-    sent(x1.at[pl.ds(0, hops)], ag1_send)
-    sent(s1, rs1_send)
-    sent(x2.at[pl.ds(0, wide - 1)], ag2_send)
     sent(s2, rs2_send)
-    for mat in range(3):
-        sent(relay[mat], rel_send.at[mat])
-        sent(relay[mat], fin_send.at[mat])
-        for w in range(3):
-            sent(many(w, mat, y_hops), y_send.at[w * 3 + mat])
-            sent(many(w, mat, n_y), sib_send.at[w * 3 + mat])
 
 
 def solution(mesh):
@@ -410,8 +469,8 @@
                 dma,
                 dma,
                 dma,
-                dma((9,)),
-                dma((9,)),
+                dma((3,)),
+                dma((3,)),
                 dma((3,)),
                 dma((3,)),
                 pltpu.SemaphoreType.REGULAR,

time: 159 us -> 155 us (0.975)
  Pallas kernels: 158 us -> 154 us
    pallas_call x1, Pallas kernels: 158 us -> 154 us  [local(): pl.pallas_call(functools.partial(kernel, n_x, n_y), out_shape=pltpu.VMEM(...]
where the time goes in v4:
time: 155 us
  Pallas kernels  154 us (99%)
    pallas_call x1, Pallas kernels, local(): pl.pallas_call(functools.partial(kernel, n_x, n_y), out_shape=pltpu.VMEM(...  154 us

profile of v4, /device:TPU:514, one launch (start us, length us, event | category | flops | bytes accessed | tf_op | source)
XLA Modules:
  0.0 154.9 jit_solution(2140043488830059668)
XLA Ops:
  0.0 154.1 %shard_map.91 = bf16[128,2048]{1,0:T(8,128)(2,1)S(1)} custom-call(bf16[128,2048]{1,0:T(8,128)(2,1)} %stream.1, bf16[16,128]{1,0:T(8,128)(2,1)} %bitcast.2, bf16[128,512]{1,0:T(8,128)(2,1)} %g1.1, bf16[128,512]{1,0:T(8,128)(2,1)} %u1_.1, bf16[512,128]{1,0:T(8,128)(2,1)} %d1.1, bf16[16,128]{1,0:T(8,128)(2,1)} %bitcast.3, bf16[128,512]{1,0:T(8,128)(2,1)} %g2.1, ...), custom_call_target="tpu_custom_call" | custom-call | tf_op jit(solution)/shard_map/pallas_call | solution.py:436
  154.1 0.8 copy.11

commit v5 on v4

--- a/solution.py
+++ b/solution.py
@@ -25,8 +25,8 @@
     stream, gain1, g1, u1, d1, gain2, g2, u2, d2,
     out,
     wg, wu, wd, st, x1, p1, s1, mid, x2, p2, s2, rg, ru, rd, hid, gains,
-    load_sem, ag1_recv, rs1_recv, ag2_recv, rs2_recv, y_recv, sib_recv, rel_recv, fin_recv,
-    ag1_send, rs1_send, ag2_send, rs2_send, y_send, sib_send, rel_send, fin_send, both_in,
+    load_sem, tok_recv, y_recv, sib_recv, rel_recv, fin_recv,
+    ag1_send, rs1_send, ag2_send, rs2_send, y_send, sib_send, rel_send, fin_send, both_in, leap_in,
 ):
     x = lax.axis_index("tp")
     f = lax.axis_index("fs")
@@ -43,7 +43,6 @@
 
     x_near = ({"tp": (x + 1) % n_x}, {"tp": (x - 1 + n_x) % n_x})
     x_leap = {"tp": (x + leap * d + n_x) % n_x}
-    x_leap_back = {"tp": (x - leap * d + n_x) % n_x}
     y_next = {"fs": CORES * ((y + d + n_y) % n_y) + c}
     y_prev = {"fs": CORES * ((y - d + n_y) % n_y) + c}
     sibling = {"fs": CORES * y + 1 - c}
@@ -96,8 +95,7 @@
 
     barrier = pltpu.get_barrier_semaphore()
     partners = [x_near[0], x_near[1], y_next, y_prev]
-    if leap > 1:
-        partners += [x_leap, x_leap_back]
+    assert leap <= 2
     for device in partners:
         pl.semaphore_signal(barrier, inc=1, device_id=device, device_id_type=MESH)
 
@@ -117,6 +115,7 @@
         for j in range(gain.shape[0]):
             gains[i, :, j * LANES:(j + 1) * LANES] = gain[j:j + 1, :].astype(F32)
     pl.semaphore_wait(barrier, len(partners) + 1 - c)
+    pl.semaphore_signal(leap_in, inc=1, device_id={"tp": (x - d + n_x) % n_x}, device_id_type=MESH)
 
     @pl.when(c == 0)
     def _():
@@ -195,7 +194,7 @@
             remote(ref, ref, sib_send.at[mat], sib_recv.at[w * 3 + mat], sibling).wait_recv()
 
     def ag1_copy(k, m):
-        return Halves(x1, k, x1, k + 1, m, ag1_send, ag1_recv, k * SUBS + m)
+        return Halves(x1, k, x1, k + 1, m, ag1_send, tok_recv, k * SUBS + m)
 
     loads[0].wait()
     for m in range(SUBS):
@@ -208,6 +207,7 @@
                 own(item)
 
     relay = (rg, ru, rd)
+    pl.semaphore_wait(leap_in, 1)
     for mat in range(3):
         if mat:
             loads[4 + mat].wait()
@@ -291,7 +291,7 @@
             ).astype(BF16)
 
     def rs1_copy(src, src_k, k, m):
-        return Halves(src, src_k, s1, k - 1, m, rs1_send, rs1_recv, (k - 1) * SUBS + m)
+        return Halves(src, src_k, s1, k - 1, m, rs1_send, tok_recv, (k - 1) * SUBS + m)
 
     def reduce_first(j, n):
         for m in range(SUBS):
@@ -321,7 +321,7 @@
 
     def ag2_copy(t):
         k, m = t // SUBS, t % SUBS
-        return Halves(x2, k, x2, k + 1, m, ag2_send, ag2_recv, t)
+        return Halves(x2, k, x2, k + 1, m, ag2_send, tok_recv, t)
 
     for m in range(SUBS):
         part = pl.ds(m * sub, sub)
@@ -350,8 +350,8 @@
     def second_quarter(k, m, lo_row, count):
         tokens = pl.ds(lo_row, count)
         if m < 2:
-            width = ff // 2
-            for lo in (0, width):
+            width = ff // 2 if count == rows else ff
+            for lo in range(0, ff, width):
                 hid[m, tokens, lo:lo + width] = hidden_part(x2[k, tokens, :], 1 + m, lo, width)
         else:
             width = feats // 2
@@ -367,7 +367,7 @@
         second_quarter(wide - 2, q, 0, rows)
 
     def rs2_copy(src, k, m):
-        return Halves(src, k, s2, k - 1, m, rs2_send, rs2_recv, (k - 1) * SUBS + m, back=True)
+        return Halves(src, k, s2, k - 1, m, rs2_send, tok_recv, (wide + k - 2) * SUBS + m, back=True)
 
     half = rows // 2
 
@@ -458,9 +458,6 @@
                 pltpu.VMEM((2, 1, feats), F32),
                 dma((7,)),
                 dma(((n_x - 1) * SUBS,)),
-                dma(((n_x - 1) * SUBS,)),
-                dma(((wide - 1) * SUBS,)),
-                dma(((wide - 1) * SUBS,)),
                 dma((y_count,)),
                 dma((9,)),
                 dma((3,)),
@@ -473,6 +470,7 @@
                 dma((3,)),
                 dma((3,)),
                 dma((3,)),
+                pltpu.SemaphoreType.REGULAR,
                 pltpu.SemaphoreType.REGULAR,
             ],
             compiler_params=pltpu.CompilerParams(

time: 155 us -> 153 us (0.987)
  Pallas kernels: 154 us -> 152 us
    pallas_call x1, Pallas kernels: 154 us -> 152 us  [local(): pl.pallas_call(functools.partial(kernel, n_x, n_y), out_shape=pltpu.VMEM(...]
where the time goes in v5:
time: 153 us
  Pallas kernels  152 us (99%)
    pallas_call x1, Pallas kernels, local(): pl.pallas_call(functools.partial(kernel, n_x, n_y), out_shape=pltpu.VMEM(...  152 us

profile of v5, /device:TPU:514, one launch (start us, length us, event | category | flops | bytes accessed | tf_op | source)
XLA Modules:
  0.0 152.8 jit_solution(2282516879843375494)
XLA Ops:
  0.0 152.0 %shard_map.91 = bf16[128,2048]{1,0:T(8,128)(2,1)S(1)} custom-call(bf16[128,2048]{1,0:T(8,128)(2,1)} %stream.1, bf16[16,128]{1,0:T(8,128)(2,1)} %bitcast.2, bf16[128,512]{1,0:T(8,128)(2,1)} %g1.1, bf16[128,512]{1,0:T(8,128)(2,1)} %u1_.1, bf16[512,128]{1,0:T(8,128)(2,1)} %d1.1, bf16[16,128]{1,0:T(8,128)(2,1)} %bitcast.3, bf16[128,512]{1,0:T(8,128)(2,1)} %g2.1, ...), custom_call_target="tpu_custom_call" | custom-call | tf_op jit(solution)/shard_map/pallas_call | solution.py:436
  152.0 0.8 copy.11

commit v6 on v5

--- a/solution.py
+++ b/solution.py
@@ -24,7 +24,7 @@
     n_x, n_y,
     stream, gain1, g1, u1, d1, gain2, g2, u2, d2,
     out,
-    wg, wu, wd, st, x1, p1, s1, mid, x2, p2, s2, rg, ru, rd, hid, gains,
+    wg, wu, wd, st, x1, p1, s1, mid, x2, p2, s2, rg, ru, rd, hid, raw, gains,
     load_sem, tok_recv, y_recv, sib_recv, rel_recv, fin_recv,
     ag1_send, rs1_send, ag2_send, rs2_send, y_send, sib_send, rel_send, fin_send, both_in, leap_in,
 ):
@@ -109,11 +109,20 @@
         ((g1, 0, 0), (u1, 0, 1), (d1, 0, 2), (g2, 1, 0), (u2, 1, 1), (d2, 1, 2))
     ):
         loads.append(pltpu.make_async_copy(src, piece(w, mat, f), load_sem.at[1 + i]))
+    for i, gain in enumerate((gain1, gain2)):
+        loads.append(pltpu.make_async_copy(gain, raw.at[i], load_sem.at[7 + i]))
     for copy in loads:
         copy.start()
-    for i, gain in enumerate((gain1, gain2)):
-        for j in range(gain.shape[0]):
-            gains[i, :, j * LANES:(j + 1) * LANES] = gain[j:j + 1, :].astype(F32)
+
+    loads[7].wait()
+    loads[8].wait()
+    for i in range(2):
+        for j in range(raw.shape[1]):
+            gains[i, :, j * LANES:(j + 1) * LANES] = raw[i, j:j + 1, :].astype(F32)
+    loads[0].wait()
+    for m in range(SUBS):
+        part = pl.ds(m * sub, sub)
+        x1[0, part, :] = rms_norm(st[part, :].astype(F32), gains[0])
     pl.semaphore_wait(barrier, len(partners) + 1 - c)
     pl.semaphore_signal(leap_in, inc=1, device_id={"tp": (x - d + n_x) % n_x}, device_id_type=MESH)
 
@@ -196,10 +205,7 @@
     def ag1_copy(k, m):
         return Halves(x1, k, x1, k + 1, m, ag1_send, tok_recv, k * SUBS + m)
 
-    loads[0].wait()
     for m in range(SUBS):
-        part = pl.ds(m * sub, sub)
-        x1[0, part, :] = rms_norm(st[part, :].astype(F32), gains[0])
         ag1_copy(0, m).start()
         if m == 0:
             for item in range(head):
@@ -436,8 +442,7 @@
         return pl.pallas_call(
             functools.partial(kernel, n_x, n_y),
             out_shape=pltpu.VMEM((rows, feats), BF16),
-            in_specs=[any_spec, vmem_spec, any_spec, any_spec, any_spec,
-                      vmem_spec, any_spec, any_spec, any_spec],
+            in_specs=[any_spec] * 9,
             out_specs=vmem_spec,
             scratch_shapes=[
                 pltpu.VMEM((3, feats, ff), BF16),
@@ -455,8 +460,9 @@
                 pltpu.VMEM((shard, ff), BF16),
                 pltpu.VMEM((ff, shard), BF16),
                 pltpu.VMEM((2, rows, ff), BF16),
+                pltpu.VMEM((2, feats // LANES, LANES), BF16),
                 pltpu.VMEM((2, 1, feats), F32),
-                dma((7,)),
+                dma((9,)),
                 dma(((n_x - 1) * SUBS,)),
                 dma((y_count,)),
                 dma((9,)),

time: 153 us -> 152 us (level)
  no operation moved by 1% of the time
where the time goes in v6:
time: 152 us
  Pallas kernels  151 us (99%)
    pallas_call x1, Pallas kernels, local(): pl.pallas_call(functools.partial(kernel, n_x, n_y), out_shape=pltpu.VMEM(...  151 us

profile of v6, /device:TPU:514, one launch (start us, length us, event | category | flops | bytes accessed | tf_op | source)
XLA Modules:
  0.0 152.0 jit_solution(15600696589211016872)
XLA Ops:
  0.0 151.2 %shard_map.91 = bf16[128,2048]{1,0:T(8,128)(2,1)S(1)} custom-call(bf16[128,2048]{1,0:T(8,128)(2,1)} %stream.1, bf16[16,128]{1,0:T(8,128)(2,1)} %bitcast.2, bf16[128,512]{1,0:T(8,128)(2,1)} %g1.1, bf16[128,512]{1,0:T(8,128)(2,1)} %u1_.1, bf16[512,128]{1,0:T(8,128)(2,1)} %d1.1, bf16[16,128]{1,0:T(8,128)(2,1)} %bitcast.3, bf16[128,512]{1,0:T(8,128)(2,1)} %g2.1, ...), custom_call_target="tpu_custom_call" | custom-call | tf_op jit(solution)/shard_map/pallas_call | solution.py:442
  151.2 0.8 copy.11
